TPU v7x, 32 devices: a whole 2x2x4 slice. The times are simulated.
32 devices in a mesh: kv: 4 (over y, x), tp: 8 (over z, core).
Axes of the slice: x: 2, y: 2, z: 4, core: 2. Of those that a mesh axis runs over, the one named last changes fastest.
Arguments:
- stream: bfloat16 [32, 4096], P(None, ('kv', 'tp')), may hold values from -18 to 18
- mixer_gain: float32 [4096], replicated, may hold values from 0.1 to 1.9
- query_weight: bfloat16 [4096, 1024], P(None, 'tp'), may hold values from -0.09375 to 0.09375
- key_weight: bfloat16 [4096, 1024], P(None, 'tp'), may hold values from -0.09375 to 0.09375
- value_weight: bfloat16 [4096, 1024], P(None, 'tp'), may hold values from -0.09375 to 0.09375
- forget_weight: bfloat16 [4096, 16], replicated, may hold values from -0.09375 to 0.09375
- forget_bias: float32 [16], replicated, may hold values from -4 to -2
- key_cache: bfloat16 [32, 16, 4096, 64], P(None, 'tp', 'kv'), may hold values from -512 to 512, as said below
- value_cache: bfloat16 [32, 16, 4096, 64], P(None, 'tp', 'kv'), may hold values from -12 to 12
- past_decay: float32 [32, 16, 4096], P(None, 'tp', 'kv'), may hold values from -4096 to 0, as said below
- out_weight: bfloat16 [1024, 4096], P('tp', 'kv'), may hold values from -0.75 to 0.75
- channel_gain: float32 [4096], replicated, may hold values from 0.1 to 1.9
- up_weight: bfloat16 [4096, 16384], P('kv', 'tp'), may hold values from -0.09375 to 0.09375
- down_weight: bfloat16 [16384, 4096], P('tp', 'kv'), may hold values from -0.0625 to 0.0625
Outputs:
- updated: bfloat16 [32, 4096], P(None, ('kv', 'tp'))
Inputs may be any that keep to these rules, and one draw needn't show every extreme that they name: `key_cache`: keys of order one; some cached keys may be much larger. `past_decay`: never falling along the positions of a sequence and head, zero at the last cached position.
All inputs are finite; a program needn't handle non-finite values.
Results may differ from a plain program's by a relative error of at most 0.014.
The roundings to bfloat16 on the way count: a program that leaves them out, or rounds other values in their place, can miss the bound.
Values may be sent and summed in bfloat16 or wider, within the bound.
No kernel may reach another device: no remote copies, remote signals or barrier semaphores. Data moves between devices by JAX's collectives and lax.ppermute only.
A program may use at most 64 MiB of HBM per device.

v0:
```python
import jax
import jax.numpy as jnp
from jax import lax
from jax.sharding import PartitionSpec as P

D = 4096
EPS = 1e-06


def combined_all(part, axis, combine):
    gathered = jax.tree.map(lambda a: lax.all_gather(a, axis), part)

    def take(source):
        return jax.tree.map(lambda a: lax.dynamic_index_in_dim(a, source, 0, False), gathered)

    return lax.fori_loop(
        1, lax.axis_size(axis), lambda source, state: combine(state, take(source)), take(0)
    )


def rms_scale(values, gain):
    widened = values.astype(jnp.float32)
    inverse = lax.rsqrt(jnp.mean(widened * widened, axis=-1, keepdims=True) + EPS)
    return (widened * inverse * gain).astype(jnp.bfloat16)


def merge_parts(earlier, later):
    top_one, total_one, sums_one = earlier
    top_two, total_two, sums_two = later
    highest = jnp.maximum(top_one, top_two)
    factor_one = jnp.exp(top_one - highest)
    factor_two = jnp.exp(top_two - highest)
    return (
        highest,
        total_one * factor_one + total_two * factor_two,
        sums_one * factor_one[..., None] + sums_two * factor_two[..., None],
    )


def squared_relu(values):
    return jnp.square(jax.nn.relu(values)).astype(jnp.bfloat16)


def row_squares(values):
    widened = values.astype(jnp.float32)
    return jnp.sum(widened * widened, axis=1)


def shards(
    stream,
    mixer_gain,
    query_weight,
    key_weight,
    value_weight,
    forget_weight,
    forget_bias,
    key_cache,
    value_cache,
    past_decay,
    out_weight,
    channel_gain,
    up_weight,
    down_weight,
):
    batch_rows = stream.shape[0]
    local_heads = key_cache.shape[1]
    head_size = key_cache.shape[3]
    scale_factor = float(head_size) ** (-0.5)
    gathered = lax.all_gather(stream, ("kv", "tp"), axis=1, tiled=True)
    normed = rms_scale(gathered, mixer_gain)
    queries = jnp.dot(normed, query_weight, preferred_element_type=jnp.float32).astype(jnp.bfloat16)
    keys_new = jnp.dot(normed, key_weight, preferred_element_type=jnp.float32).astype(jnp.bfloat16)
    values_new = jnp.dot(normed, value_weight, preferred_element_type=jnp.float32).astype(
        jnp.bfloat16
    )
    forget_all = jax.nn.log_sigmoid(
        jnp.dot(normed, forget_weight, preferred_element_type=jnp.float32) + forget_bias
    )
    forget = lax.dynamic_slice_in_dim(
        forget_all, lax.axis_index("tp") * local_heads, local_heads, 1
    )
    query_heads = queries.reshape(batch_rows, local_heads, head_size)
    scores = (
        jnp.einsum("bhd,bhpd->bhp", query_heads, key_cache, preferred_element_type=jnp.float32)
        * scale_factor
        + forget[..., None]
        + past_decay
    )
    highest = jnp.max(scores, axis=-1)
    weights = jnp.exp(scores - highest[..., None]).astype(jnp.bfloat16)
    totals = jnp.sum(weights.astype(jnp.float32), axis=-1)
    sums = jnp.einsum("bhp,bhpd->bhd", weights, value_cache, preferred_element_type=jnp.float32)
    highest, totals, sums = combined_all((highest, totals, sums), "kv", merge_parts)
    key_heads = keys_new.reshape(batch_rows, local_heads, head_size).astype(jnp.float32)
    value_heads = values_new.reshape(batch_rows, local_heads, head_size).astype(jnp.float32)
    own = jnp.sum(query_heads.astype(jnp.float32) * key_heads, axis=-1) * scale_factor
    peak = jnp.maximum(highest, own)
    cache_factor = jnp.exp(highest - peak)
    own_factor = jnp.exp(own - peak)
    numer = sums * cache_factor[..., None] + value_heads * own_factor[..., None]
    denom = totals * cache_factor + own_factor
    attention = (
        (numer / denom[..., None]).astype(jnp.bfloat16).reshape(batch_rows, local_heads * head_size)
    )
    partial_value = jnp.dot(attention, out_weight, preferred_element_type=jnp.float32)
    piece_width = stream.shape[1]
    block_width = partial_value.shape[1]
    block_sum = lax.psum(partial_value, "tp")
    own_block = lax.dynamic_slice_in_dim(
        gathered, lax.axis_index("kv") * block_width, block_width, 1
    )
    middle_block = (own_block.astype(jnp.float32) + block_sum).astype(jnp.bfloat16)
    squares = lax.psum(row_squares(middle_block), "kv")
    middle_piece = lax.dynamic_slice_in_dim(
        middle_block, lax.axis_index("tp") * piece_width, piece_width, 1
    )
    inverse = lax.rsqrt(squares / D + EPS)
    gain_block = lax.dynamic_slice_in_dim(
        channel_gain, lax.axis_index("kv") * block_width, block_width, 0
    )
    mixed_block = (
        middle_block.astype(jnp.float32) * inverse[:, None] * gain_block[None, :]
    ).astype(jnp.bfloat16)
    up_partial = jnp.dot(mixed_block, up_weight, preferred_element_type=jnp.float32)
    hidden = squared_relu(lax.psum(up_partial, "kv"))
    down_partial = jnp.dot(hidden, down_weight, preferred_element_type=jnp.float32)
    reduced = lax.psum_scatter(down_partial, "tp", scatter_dimension=1, tiled=True)
    return (middle_piece.astype(jnp.float32) + reduced).astype(jnp.bfloat16)


def solution(mesh):
    return jax.shard_map(
        shards,
        mesh=mesh,
        in_specs=(
            P(None, ("kv", "tp")),
            P(),
            P(None, "tp"),
            P(None, "tp"),
            P(None, "tp"),
            P(),
            P(),
            P(None, "tp", "kv", None),
            P(None, "tp", "kv", None),
            P(None, "tp", "kv"),
            P("tp", "kv"),
            P(),
            P("kv", "tp"),
            P("tp", "kv"),
        ),
        out_specs=P(None, ("kv", "tp")),
        check_vma=False,
    )
```

profile of v0, /device:TPU:0, one launch (start us, length us, event | category | flops | bytes accessed | tf_op | source)
XLA Modules:
  0.0 247.9 jit_solution(13276194251928122677)
XLA Ops:
  6.5 0.0 copy-start
  6.5 0.0 all-reduce.3.cloned.1.call-start
  6.5 44.6 %all_gather.21 = bf16[32,4096]{1,0:T(8,128)(2,1)S(1)} all-gather(bf16[32,128]{1,0:T(8,128)(2,1)} %param.16), channel_id=1, replica_groups=mesh['kv'=4,'tp'=8] {'kv','tp'}, dimensions={1}, use_global_device_ids=true | all-gather | bytes 270336 | tf_op jit(solution)/shard_map/all_gather | solution.py:69
  51.2 0.2 fusion.6
  51.3 0.0 copy-done
  51.4 1.0 convolution_convert_fusion.2
  52.4 0.1 reshape.57
  52.5 0.1 reshape.31
  52.6 1.2 fusion.40
  53.8 0.1 copy.32
  53.9 4.6 %fusion.41 = f32[32,2,1,1024]{3,2,1,0:T(1,128)S(1)} fusion(bf16[32,2,64,1]{2,3,1,0:T(2,128)(2,1)S(1)} %reshape.57, bf16[32,2,1024,64]{2,3,1,0:T(8,128)(2,1)} %param.23), kind=kOutput, calls=%fused_computation.63 | convolution fusion | flops 8388608 | bytes 8658944 | tf_op jit(solution)/shard_map/bhd,bhpd->bhp/dot_general | solution.py:84
  58.4 0.0 copy-start.1
  58.4 0.0 copy-start.4
  58.5 0.0 copy-start.2
  58.5 2.1 fusion.38
  60.5 0.1 copy.33
  60.6 1.3 fusion.30
  61.9 5.7 %fusion.11 = f32[32,2,1,64]{3,2,1,0:T(1,128)S(1)} fusion(bf16[32,2,1024,64]{2,3,1,0:T(8,128)(2,1)} %param.24, bf16[32,2,1024,1]{2,1,0,3:T(2,128)(2,1)S(1)} %get-tuple-element.211), kind=kOutput, calls=%fused_computation.24 | convolution fusion | flops 8388608 | bytes 8536064 | tf_op jit(solution)/shard_map/bhp,bhpd->bhd/dot_general | solution.py:92
  67.6 7.5 %all-gather.2 = f32[128,2,64]{2,1,0:T(2,128)S(1)} all-gather(f32[32,2,64]{2,1,0:T(2,128)S(1)} %bitcast.49), channel_id=4, replica_groups=mesh['kv'=4,'tp'=8] {'kv'}, dimensions={0}, use_global_device_ids=true | all-gather | bytes 81920 | tf_op jit(solution)/shard_map/all_gather | solution.py:11
  75.0 0.0 copy-start.3
  75.0 0.6 copy-done.3
  75.7 0.1 copy.34
  75.8 8.1 %all-gather.4 = f32[4,32,2]{1,2,0:T(2,128)S(1)} all-gather(f32[1,32,2]{1,2,0:T(2,128)S(1)} %bitcast.51), channel_id=3, replica_groups=mesh['kv'=4,'tp'=8] {'kv'}, dimensions={0}, use_global_device_ids=true | all-gather | bytes 1280 | tf_op jit(solution)/shard_map/all_gather | solution.py:11
  83.8 7.1 %all-gather.3 = f32[4,32,2]{1,2,0:T(2,128)S(1)} all-gather(f32[1,32,2]{1,2,0:T(2,128)S(1)} %bitcast.50), channel_id=2, replica_groups=mesh['kv'=4,'tp'=8] {'kv'}, dimensions={0}, use_global_device_ids=true | all-gather | bytes 1280 | tf_op jit(solution)/shard_map/all_gather | solution.py:11
  90.9 3.6 %while.19 = (s32[]{:T(128)}, f32[32,2]{0,1:T(2,128)S(1)}, f32[32,2]{0,1:T(2,128)S(1)}, f32[32,2,64]{2,1,0:T(2,128)S(1)}, f32[4,32,2]{1,2,0:T(2,128)S(1)}, /*inde...) while((s32[]{:T(128)}, f32[32,2]{0,1:T(2,128)S(1)}, ...), condition=%wide.region_4.5_spmd, body=%wide.region_3.4_spmd.sunk | while | flops 12677 | bytes 52887 | solution.py:16
  90.9 0.1 copy.49
  91.0 0.1 copy.50
  91.1 1.0 fusion.57
  92.2 0.1 copy.49
  92.2 0.1 copy.50
  92.3 1.0 fusion.57
  93.4 0.1 copy.49
  93.5 0.1 copy.50
  93.5 1.0 fusion.57
  94.5 0.0 copy-done.1
  94.5 0.0 copy-done.4
  94.6 0.3 fusion.4
  94.9 0.1 reshape.33
  95.0 0.1 multiply_reduce_fusion
  95.1 0.1 copy.35
  95.2 0.1 copy.36
  95.3 0.1 copy.37
  95.4 0.1 copy.38
  95.5 0.0 copy-done.2
  95.5 0.3 fusion.3
  95.8 0.1 reshape.34
  95.9 0.2 fusion.22
  96.1 0.1 reshape.32
  96.2 1.8 fusion.42
  97.9 0.0 all-reduce.3.cloned.1.call-update
  98.0 0.0 all-reduce.5.cloned.1.call-start
  98.0 0.7 dynamic_slice.59
  98.7 51.7 %all-reduce.3.cloned.1.call-done = f32[32,1024]{1,0:T(8,128)} async-done(((f32[32,1024]{1,0:T(8,128)}), f32[32,1024]{1,0:T(8,128)}) %all-reduce.3.cloned.1.call-update) | async-done | bytes 131088 | tf_op jit(solution)/shard_map/psum | solution.py:108
  150.4 1.0 fusion.13
  151.4 9.8 %psum.22 = f32[32]{0:T(128)S(1)} all-reduce(f32[32]{0:T(128)S(1)} %get-tuple-element.204), channel_id=1, replica_groups=mesh['kv'=4,'tp'=8] {'kv'}, use_global_device_ids=true, to_apply=%region_8.9 | all-reduce | flops 32 | bytes 256 | tf_op jit(solution)/shard_map/psum | solution.py:113
  161.3 3.8 %fusion.18 = f32[32,2048]{1,0:T(8,128)} fusion(bf16[1024,2048]{1,0:T(8,128)(2,1)} %param.28, bf16[32,1024]{1,0:T(8,128)(2,1)S(1)} %get-tuple-element.205, f32[1024]{0:T(1024)S(1)} %dynamic_slice.59, f32[32]{0:T(128)S(1)} %add_rsqrt_fusion), kind=kOutput, calls=%fused_computation.37 | convolution fusion | flops 134348800 | bytes 4526208 | tf_op jit(solution)/shard_map/dot_general | solution.py:124
  165.0 0.0 all-reduce.5.cloned.1.call-update
  165.1 0.0 reduce-scatter.2.cloned.1.call-start
  165.1 40.4 %all-reduce.5.cloned.1.call-done = f32[32,2048]{1,0:T(8,128)} async-done(((f32[32,2048]{1,0:T(8,128)}), f32[32,2048]{1,0:T(8,128)}) %all-reduce.5.cloned.1.call-update) | async-done | bytes 262160 | tf_op jit(solution)/shard_map/psum | solution.py:125
  205.5 3.8 %fusion.16 = f32[32,1024]{1,0:T(8,128)} fusion(bf16[2048,1024]{1,0:T(8,128)(2,1)} %param.29, f32[32,2048]{1,0:T(8,128)} %all-reduce.5.cloned.1.call-done), kind=kOutput, calls=%fused_computation.34 | convolution fusion | flops 134414336 | bytes 4587520 | tf_op jit(solution)/shard_map/dot_general | solution.py:126
  209.3 0.0 reduce-scatter.2.cloned.1.call-update
  209.3 30.7 %reduce-scatter.2.cloned.1.call-done = f32[32,128]{1,0:T(8,128)} async-done(((f32[32,1024]{1,0:T(8,128)}), f32[32,128]{1,0:T(8,128)}) %reduce-scatter.2.cloned.1.call-update) | async-done | bytes 16400 | tf_op jit(solution)/shard_map/reduce_scatter | solution.py:127
  240.0 1.3 add_convert_fusion.1
  (10 shorter events, 0.1 us)
Async XLA Ops:
  6.5 44.8 %copy-start = (bf16[4096,128]{1,0:T(8,128)(2,1)S(1)}, bf16[4096,128]{1,0:T(8,128)(2,1)}, u32[]{:S(2)}) copy-start(bf16[4096,128]{1,0:T(8,128)(2,1)} %param.18) | copy-start | bytes 3145732
  6.5 143.8 %all-reduce.3.cloned.1.call-start = ((), (), s32[]{:S(2)}) async-start(), calls=%async_computation.1 | async-start | bytes 262144 | tf_op jit(solution)/shard_map/psum | solution.py:108
  58.4 36.1 %copy-start.1 = (bf16[4096,128]{1,0:T(8,128)(2,1)S(1)}, bf16[4096,128]{1,0:T(8,128)(2,1)}, u32[]{:S(2)}) copy-start(bf16[4096,128]{1,0:T(8,128)(2,1)} %param.19) | copy-start | bytes 3145732
  58.4 36.1 %copy-start.4 = (f32[4096]{0:T(1024)S(1)}, f32[4096]{0:T(1024)}, u32[]{:S(2)}) copy-start(f32[4096]{0:T(1024)} %param.17) | copy-start | bytes 49156
  58.5 37.0 %copy-start.2 = (bf16[4096,128]{1,0:T(8,128)(2,1)S(1)}, bf16[4096,128]{1,0:T(8,128)(2,1)}, u32[]{:S(2)}) copy-start(bf16[4096,128]{1,0:T(8,128)(2,1)} %param.20) | copy-start | bytes 3145732
  75.0 0.6 copy-start.3
  98.0 107.5 %all-reduce.5.cloned.1.call-start = ((), (), s32[]{:S(2)}) async-start(), calls=%async_computation.2 | async-start | bytes 524288 | tf_op jit(solution)/shard_map/psum | solution.py:125
  165.1 75.0 %reduce-scatter.2.cloned.1.call-start = ((), (), s32[]{:S(2)}) async-start(), calls=%async_computation.3 | async-start | bytes 147456 | tf_op jit(solution)/shard_map/reduce_scatter | solution.py:127
Sparse Core Ops, SparseCore 0:
  98.1 52.2 all-reduce.2
  165.2 40.2 all-reduce.4
  209.4 30.5 reduce-scatter.1
where the time goes:
time: 249 us; the launch traced here: 248 us
  waiting for transfers between devices  123 us (49%)
  blocking collectives  77.1 us (31%)
  matrix products  22.4 us (9%)
  between operations  13.2 us (5%)
  other arithmetic  9.28 us (4%)
  local copies, waits for them, and re-layouts  2.9 us (1%)
    psum x1, waiting for transfers between devices, shards(): block_sum = lax.psum(partial_value, 'tp')  51.7 us
    all_gather x1, blocking collectives, shards(): gathered = lax.all_gather(stream, ('kv', 'tp'), axis=1, tiled=True)  44.6 us
    psum x1, waiting for transfers between devices, shards(): hidden = squared_relu(lax.psum(up_partial, 'kv'))  40.4 us
    reduce_scatter x1, waiting for transfers between devices, shards(): lax.psum_scatter(down_partial, 'tp', scatter_dimension=1, tiled=True)  30.7 us
    all_gather x3, blocking collectives, combined_all(): gathered = jax.tree.map(lambda a: lax.all_gather(a, axis), part)  22.6 us
    psum x1, blocking collectives, shards(): squares = lax.psum(row_squares(middle_block), 'kv')  9.84 us
    dot_general x1, matrix products, shards(): jnp.einsum('bhp,bhpd->bhd', weights, value_cache, preferred_element_type=...  5.65 us
  transfers between devices with their start and end apart: 3, of which 3 were waited for; matrix products, arithmetic and copies ran while one was open for 0% of the time, Pallas kernels for 0%

commit v1 on v0

--- a/solution.py
+++ b/solution.py
@@ -105,7 +105,11 @@
     partial_value = jnp.dot(attention, out_weight, preferred_element_type=jnp.float32)
     piece_width = stream.shape[1]
     block_width = partial_value.shape[1]
-    block_sum = lax.psum(partial_value, "tp")
+    block_sum = partial_value
+    for hop in (1, 2, 4):
+        block_sum = block_sum + lax.ppermute(
+            block_sum, "tp", [(dev, dev ^ hop) for dev in range(8)]
+        )
     own_block = lax.dynamic_slice_in_dim(
         gathered, lax.axis_index("kv") * block_width, block_width, 1
     )

time: 249 us -> 210 us (0.84)
  waiting for transfers between devices: 123 us -> 85.7 us
    psum x1 -> x0, waiting for transfers between devices: 51.7 us -> none  [shards(): block_sum = lax.psum(partial_value, 'tp')]
    ppermute x0 -> x3, waiting for transfers between devices: none -> 14.6 us  [shards(): lax.ppermute(block_sum, 'tp', [(dev, dev ^ hop) for dev in range(8)])]
  transfers between devices with their start and end apart: 3 -> 5, of which waited for: 3 -> 5; matrix products, arithmetic and copies ran while one was open for 0% -> 0% of each run, Pallas kernels for 0% -> 0%
where the time goes in v1:
time: 210 us; the launch traced here: 209 us
  waiting for transfers between devices  85.7 us (41%)
  blocking collectives  76.2 us (36%)
  matrix products  21.7 us (10%)
  between operations  13.6 us (6%)
  other arithmetic  8.41 us (4%)
  local copies, waits for them, and re-layouts  2.9 us (1%)
    all_gather x1, blocking collectives, shards(): gathered = lax.all_gather(stream, ('kv', 'tp'), axis=1, tiled=True)  44.6 us
    psum x1, waiting for transfers between devices, shards(): hidden = squared_relu(lax.psum(up_partial, 'kv'))  40.4 us
    reduce_scatter x1, waiting for transfers between devices, shards(): lax.psum_scatter(down_partial, 'tp', scatter_dimension=1, tiled=True)  30.7 us
    all_gather x3, blocking collectives, combined_all(): gathered = jax.tree.map(lambda a: lax.all_gather(a, axis), part)  22.6 us
    ppermute x3, waiting for transfers between devices, shards(): lax.ppermute(block_sum, 'tp', [(dev, dev ^ hop) for dev in range(8)])  14.6 us
    psum x1, blocking collectives, shards(): squares = lax.psum(row_squares(middle_block), 'kv')  8.98 us
    dot_general x1, matrix products, shards(): jnp.einsum('bhp,bhpd->bhd', weights, value_cache, preferred_element_type=...  5.65 us
    dot_general x1, matrix products, shards(): jnp.einsum('bhd,bhpd->bhp', query_heads, key_cache, preferred_element_typ...  4.59 us
  transfers between devices with their start and end apart: 5, of which 5 were waited for; matrix products, arithmetic and copies ran while one was open for 0% of the time, Pallas kernels for 0%

profile of v1, /device:TPU:0, one launch (start us, length us, event | category | flops | bytes accessed | tf_op | source)
XLA Modules:
  0.0 208.8 jit_solution(2053224941343637644)
XLA Ops:
  6.5 0.0 copy-start
  6.5 0.0 all-reduce.2.cloned.1.call-start
  6.5 44.6 %all_gather.21 = bf16[32,4096]{1,0:T(8,128)(2,1)S(1)} all-gather(bf16[32,128]{1,0:T(8,128)(2,1)} %param.16), channel_id=1, replica_groups=mesh['kv'=4,'tp'=8] {'kv','tp'}, dimensions={1}, use_global_device_ids=true | all-gather | bytes 270336 | tf_op jit(solution)/shard_map/all_gather | solution.py:69
  51.2 0.2 fusion.6
  51.3 0.0 copy-done
  51.4 1.0 convolution_convert_fusion.2
  52.4 0.1 reshape.57
  52.5 0.1 reshape.31
  52.6 1.2 fusion.40
  53.8 0.1 copy.32
  53.9 4.6 %fusion.41 = f32[32,2,1,1024]{3,2,1,0:T(1,128)S(1)} fusion(bf16[32,2,64,1]{2,3,1,0:T(2,128)(2,1)S(1)} %reshape.57, bf16[32,2,1024,64]{2,3,1,0:T(8,128)(2,1)} %param.23), kind=kOutput, calls=%fused_computation.63 | convolution fusion | flops 8388608 | bytes 8658944 | tf_op jit(solution)/shard_map/bhd,bhpd->bhp/dot_general | solution.py:84
  58.4 0.0 copy-start.1
  58.5 0.0 copy-start.2
  58.5 2.1 fusion.38
  60.5 0.1 copy.33
  60.6 1.3 fusion.30
  61.9 5.7 %fusion.11 = f32[32,2,1,64]{3,2,1,0:T(1,128)S(1)} fusion(bf16[32,2,1024,64]{2,3,1,0:T(8,128)(2,1)} %param.24, bf16[32,2,1024,1]{2,1,0,3:T(2,128)(2,1)S(1)} %get-tuple-element.211), kind=kOutput, calls=%fused_computation.24 | convolution fusion | flops 8388608 | bytes 8536064 | tf_op jit(solution)/shard_map/bhp,bhpd->bhd/dot_general | solution.py:92
  67.6 7.5 %all-gather.2 = f32[128,2,64]{2,1,0:T(2,128)S(1)} all-gather(f32[32,2,64]{2,1,0:T(2,128)S(1)} %bitcast.49), channel_id=4, replica_groups=mesh['kv'=4,'tp'=8] {'kv'}, dimensions={0}, use_global_device_ids=true | all-gather | bytes 81920 | tf_op jit(solution)/shard_map/all_gather | solution.py:11
  75.0 0.6 copy-done.3
  75.7 0.1 copy.34
  75.8 8.1 %all-gather.4 = f32[4,32,2]{1,2,0:T(2,128)S(1)} all-gather(f32[1,32,2]{1,2,0:T(2,128)S(1)} %bitcast.51), channel_id=3, replica_groups=mesh['kv'=4,'tp'=8] {'kv'}, dimensions={0}, use_global_device_ids=true | all-gather | bytes 1280 | tf_op jit(solution)/shard_map/all_gather | solution.py:11
  83.8 7.1 %all-gather.3 = f32[4,32,2]{1,2,0:T(2,128)S(1)} all-gather(f32[1,32,2]{1,2,0:T(2,128)S(1)} %bitcast.50), channel_id=2, replica_groups=mesh['kv'=4,'tp'=8] {'kv'}, dimensions={0}, use_global_device_ids=true | all-gather | bytes 1280 | tf_op jit(solution)/shard_map/all_gather | solution.py:11
  90.9 3.6 %while.19 = (s32[]{:T(128)}, f32[32,2]{0,1:T(2,128)S(1)}, f32[32,2]{0,1:T(2,128)S(1)}, f32[32,2,64]{2,1,0:T(2,128)S(1)}, f32[4,32,2]{1,2,0:T(2,128)S(1)}, /*inde...) while((s32[]{:T(128)}, f32[32,2]{0,1:T(2,128)S(1)}, ...), condition=%wide.region_4.5_spmd, body=%wide.region_3.4_spmd.sunk | while | flops 12677 | bytes 52887 | solution.py:16
  90.9 0.1 copy.49
  91.0 0.1 copy.50
  91.1 1.0 fusion.57
  92.2 0.1 copy.49
  92.2 0.1 copy.50
  92.3 1.0 fusion.57
  93.4 0.1 copy.49
  93.5 0.1 copy.50
  93.5 1.0 fusion.57
  94.5 0.0 copy-done.1
  94.5 0.0 copy-done.4
  94.6 0.3 fusion.4
  94.9 0.1 reshape.33
  95.0 0.1 multiply_reduce_fusion
  95.1 0.1 copy.35
  95.2 0.1 copy.36
  95.3 0.1 copy.37
  95.4 0.1 copy.38
  95.5 0.0 copy-done.2
  95.5 0.3 fusion.3
  95.8 0.1 reshape.34
  95.9 0.2 fusion.22
  96.1 0.1 reshape.32
  96.2 1.1 fusion.42
  97.3 0.1 collective-permute-start
  97.4 1.3 collective-permute-done
  98.7 0.1 collective-permute-start.1
  98.8 5.5 %collective-permute-done.1 = f32[32,1024]{1,0:T(8,128)S(1)} collective-permute-done((f32[32,1024]{1,0:T(8,128)S(1)}, f32[32,1024]{1,0:T(8,128)S(1)}, u32[]{:S(2)}, u32[]{:S(2)}) %collective-permute-start.1) | collective-permute-done | bytes 131104 | tf_op jit(solution)/shard_map/ppermute | solution.py:110
  104.3 0.1 collective-permute-start.2
  104.4 0.7 dynamic_slice.59
  105.1 7.7 %collective-permute-done.2 = f32[32,1024]{1,0:T(8,128)S(1)} collective-permute-done((f32[32,1024]{1,0:T(8,128)S(1)}, f32[32,1024]{1,0:T(8,128)S(1)}, u32[]{:S(2)}, u32[]{:S(2)}) %collective-permute-start.2) | collective-permute-done | bytes 131104 | tf_op jit(solution)/shard_map/ppermute | solution.py:110
  112.8 0.1 fusion.13
  113.0 9.0 %psum.14 = f32[32]{0:T(128)S(1)} all-reduce(f32[32]{0:T(128)S(1)} %get-tuple-element.204), channel_id=1, replica_groups=mesh['kv'=4,'tp'=8] {'kv'}, use_global_device_ids=true, to_apply=%region_7.8 | all-reduce | flops 32 | bytes 256 | tf_op jit(solution)/shard_map/psum | solution.py:117
  121.9 3.8 %fusion.18 = f32[32,2048]{1,0:T(8,128)} fusion(bf16[1024,2048]{1,0:T(8,128)(2,1)} %param.28, bf16[32,1024]{1,0:T(8,128)(2,1)S(1)} %get-tuple-element.205, f32[1024]{0:T(1024)S(1)} %dynamic_slice.59, f32[32]{0:T(128)S(1)} %add_rsqrt_fusion), kind=kOutput, calls=%fused_computation.37 | convolution fusion | flops 134348800 | bytes 4526208 | tf_op jit(solution)/shard_map/dot_general | solution.py:128
  125.7 0.0 all-reduce.2.cloned.1.call-update
  125.7 0.0 reduce-scatter.2.cloned.1.call-start
  125.8 40.4 %all-reduce.2.cloned.1.call-done = f32[32,2048]{1,0:T(8,128)} async-done(((f32[32,2048]{1,0:T(8,128)}), f32[32,2048]{1,0:T(8,128)}) %all-reduce.2.cloned.1.call-update) | async-done | bytes 262160 | tf_op jit(solution)/shard_map/psum | solution.py:129
  166.1 3.8 %fusion.16 = f32[32,1024]{1,0:T(8,128)} fusion(bf16[2048,1024]{1,0:T(8,128)(2,1)} %param.29, f32[32,2048]{1,0:T(8,128)} %all-reduce.2.cloned.1.call-done), kind=kOutput, calls=%fused_computation.34 | convolution fusion | flops 134414336 | bytes 4587520 | tf_op jit(solution)/shard_map/dot_general | solution.py:130
  169.9 0.0 reduce-scatter.2.cloned.1.call-update
  169.9 30.7 %reduce-scatter.2.cloned.1.call-done = f32[32,128]{1,0:T(8,128)} async-done(((f32[32,1024]{1,0:T(8,128)}), f32[32,128]{1,0:T(8,128)}) %reduce-scatter.2.cloned.1.call-update) | async-done | bytes 16400 | tf_op jit(solution)/shard_map/reduce_scatter | solution.py:131
  200.7 1.3 add_convert_fusion.1
  (14 shorter events, 0.2 us)
Async XLA Ops:
  6.5 44.8 %copy-start = (bf16[4096,128]{1,0:T(8,128)(2,1)S(1)}, bf16[4096,128]{1,0:T(8,128)(2,1)}, u32[]{:S(2)}) copy-start(bf16[4096,128]{1,0:T(8,128)(2,1)} %param.18) | copy-start | bytes 3145732
  6.5 159.6 %all-reduce.2.cloned.1.call-start = ((), (), s32[]{:S(2)}) async-start(), calls=%async_computation.1 | async-start | bytes 524288 | tf_op jit(solution)/shard_map/psum | solution.py:129
  58.4 36.1 %copy-start.1 = (bf16[4096,128]{1,0:T(8,128)(2,1)S(1)}, bf16[4096,128]{1,0:T(8,128)(2,1)}, u32[]{:S(2)}) copy-start(bf16[4096,128]{1,0:T(8,128)(2,1)} %param.19) | copy-start | bytes 3145732
  58.4 36.1 %copy-start.4 = (f32[4096]{0:T(1024)S(1)}, f32[4096]{0:T(1024)}, u32[]{:S(2)}) copy-start(f32[4096]{0:T(1024)} %param.17) | copy-start | bytes 49156
  58.5 37.0 %copy-start.2 = (bf16[4096,128]{1,0:T(8,128)(2,1)S(1)}, bf16[4096,128]{1,0:T(8,128)(2,1)}, u32[]{:S(2)}) copy-start(bf16[4096,128]{1,0:T(8,128)(2,1)} %param.20) | copy-start | bytes 3145732
  75.0 0.6 copy-start.3
  97.3 1.4 collective-permute-start
  98.7 5.6 %collective-permute-start.1 = (f32[32,1024]{1,0:T(8,128)S(1)}, f32[32,1024]{1,0:T(8,128)S(1)}, u32[]{:S(2)}, u32[]{:S(2)}) collective-permute-start(f32[32,1024]{1,0:T(8,128)S(1)} %add.148), channel_id=1, source_target_pairs={{0,2},{1,3},{2,0},{3,1},{4,6},{5,7},{6,4},{7,5},{8,10},{9,11},{10,... | collective-permute-start | bytes 393224 | tf_op jit(solution)/shard_map/ppermute | solution.py:110
  104.3 8.5 %collective-permute-start.2 = (f32[32,1024]{1,0:T(8,128)S(1)}, f32[32,1024]{1,0:T(8,128)S(1)}, u32[]{:S(2)}, u32[]{:S(2)}) collective-permute-start(f32[32,1024]{1,0:T(8,128)S(1)} %add.149), channel_id=1, source_target_pairs={{0,4},{1,5},{2,6},{3,7},{4,0},{5,1},{6,2},{7,3},{8,12},{9,13},{10,... | collective-permute-start | bytes 393224 | tf_op jit(solution)/shard_map/ppermute | solution.py:110
  125.7 74.9 %reduce-scatter.2.cloned.1.call-start = ((), (), s32[]{:S(2)}) async-start(), calls=%async_computation.2 | async-start | bytes 147456 | tf_op jit(solution)/shard_map/reduce_scatter | solution.py:131
Sparse Core Ops, SparseCore 0:
  125.8 40.2 all-reduce.1
  170.1 30.5 reduce-scatter.1
